TPU v7x, 32 devices: a whole 2x2x4 slice. The times are simulated.
32 devices in a mesh: grp: 2 (over y), kv: 4 (over z), tp: 4 (over x, core).
Axes of the slice: x: 2, y: 2, z: 4, core: 2. Of those that a mesh axis runs over, the one named last changes fastest.
Arguments:
- tokens: bfloat16 [8, 3, 4096], P(('grp', 'kv')), parts along dimension 0, may hold values from -6 to 6
- input_norm_scale: float32 [4096], replicated, may hold values from 0.1 to 1.9
- head_input_matrix: bfloat16 [4096, 8192], P('kv', 'tp'), may hold values from -0.09375 to 0.09375
- output_gate_matrix: bfloat16 [4096, 8192], P('kv', 'tp'), may hold values from -0.09375 to 0.09375
- group_input_matrix: bfloat16 [4096, 512], P('kv', 'tp'), may hold values from -0.09375 to 0.09375
- group_readout_matrix: bfloat16 [4096, 512], P('kv', 'tp'), may hold values from -0.09375 to 0.09375
- step_size_matrix: bfloat16 [4096, 128], P(None, 'tp'), may hold values from -0.09375 to 0.09375
- step_size_bias: float32 [128], P('tp'), may hold values from -4 to -1
- log_decay_rate: float32 [128], P('tp'), may hold values from -4.6 to 2
- direct_path_weight: float32 [128], P('tp'), may hold values from 0.1 to 1.9
- convolution_tap_weight: bfloat16 [4, 8, 1152], P(None, 'tp'), may hold values from -3 to 3
- convolution_history_rows: bfloat16 [8, 6, 8, 1152], P(('grp', 'kv'), None, 'tp'), parts along dimension 0, may hold values from -6 to 6
- per_proposal_states: float32 [8, 3, 128, 64, 64], P(('grp', 'kv'), None, 'tp'), parts along dimension 0, may hold values from -4 to 4
- accepted: int32 [8], P(('grp', 'kv')), parts along dimension 0, may hold values from 1 to 3
- proposal_extra_decay: float32 [8, 3, 128], P(('grp', 'kv'), None, 'tp'), parts along dimension 0, may hold values from -0.69 to 0
- group_norm_scale: float32 [8192], P('tp'), may hold values from 0.1 to 1.9
- output_projection_matrix: bfloat16 [8192, 4096], P('tp', 'kv'), may hold values from -0.0625 to 0.0625
Outputs:
- mixed: bfloat16 [8, 3, 4096], P(('grp', 'tp'), None, 'kv'), parts along dimension 0
- new_states: float32 [8, 3, 128, 64, 64], P(('grp', 'kv'), None, 'tp'), parts along dimension 0
- new_tail: bfloat16 [8, 6, 8, 1152], P(('grp', 'kv'), None, 'tp'), parts along dimension 0
There are 2 independent parts, one for each index of `grp`. A program takes and returns all parts, laid end to end along the dimension named above; an argument that names none is the same for every part. Nothing has to cross between parts.
All inputs are finite; a program needn't handle non-finite values.
Results may differ from a plain program's by a relative error of at most 0.015.
Values may be sent and summed in bfloat16 or wider, within the bound.
No kernel may reach another device: no remote copies, remote signals or barrier semaphores. Data moves between devices by JAX's collectives and lax.ppermute only.
A program may use at most 64 MiB of HBM per device.

v0:
```python
import jax
import jax.numpy as jnp
from jax import lax
from jax.sharding import PartitionSpec as P

epsilon = 1e-06


def rms_scale(values):
    return lax.rsqrt(jnp.mean(values * values, axis=-1, keepdims=True) + epsilon)


def causal_states(log_decay_factor, head_step_size, ssm_inputs, inject, start_state):
    cumulative = jnp.cumsum(log_decay_factor, axis=1)
    length = log_decay_factor.shape[1]
    lower = (jnp.arange(length)[:, None] >= jnp.arange(length)[None, :])[None, :, :, None]
    spread = cumulative[:, :, None, :] - cumulative[:, None, :, :]
    factors = jnp.where(lower, jnp.exp(jnp.where(lower, spread, 0.0)), 0.0)
    mixing = factors * head_step_size[:, None, :, :]
    carried = jnp.exp(cumulative)[..., None, None] * start_state[:, None]
    return carried + jnp.einsum("sjih,sihp,sihn->sjhpn", mixing, ssm_inputs, inject)


def combine_head_outputs(
    incoming_token_rows,
    gate_portion,
    unactivated_step,
    step_size_bias,
    log_decay_rate,
    direct_path_weight,
    convolution_tap_weight,
    convolution_history_rows,
    per_proposal_states,
    accepted,
    proposal_extra_decay,
    group_norm_scale,
):
    sequences, proposals, group_count, group_width = incoming_token_rows.shape
    head_count = step_size_bias.shape[0]
    head_dim = per_proposal_states.shape[3]
    state_size = per_proposal_states.shape[4]
    per_group = head_count // group_count
    group_inner = per_group * head_dim
    tap_count = convolution_tap_weight.shape[0]
    offsets = accepted[:, None] + jnp.arange(tap_count - 1, dtype=jnp.int32)[None, :]
    context = jnp.take_along_axis(convolution_history_rows, offsets[:, :, None, None], axis=1)
    convolution_span = jnp.concatenate([context, incoming_token_rows], axis=1)
    widened = convolution_span.astype(jnp.float32)
    convolved = jnp.zeros((sequences, proposals, group_count, group_width), jnp.float32)
    for conv_tap in range(tap_count):
        convolved = convolved + widened[
            :, conv_tap : conv_tap + proposals
        ] * convolution_tap_weight[conv_tap].astype(jnp.float32)
    activated = jax.nn.silu(convolved)
    ssm_inputs = activated[..., :group_inner].reshape(sequences, proposals, head_count, head_dim)
    inject = jnp.repeat(activated[..., group_inner : group_inner + state_size], per_group, axis=2)
    readout = jnp.repeat(activated[..., group_inner + state_size :], per_group, axis=2)
    head_step_size = jax.nn.softplus(unactivated_step + step_size_bias)
    log_decay_factor = proposal_extra_decay - jnp.exp(log_decay_rate) * head_step_size
    chosen = (accepted - 1)[:, None, None, None, None]
    start_state = jnp.take_along_axis(per_proposal_states, chosen, axis=1)[:, 0]
    running_state_rows = causal_states(
        log_decay_factor, head_step_size, ssm_inputs, inject, start_state
    )
    response = (
        jnp.einsum("sjhn,sjhpn->sjhp", readout, running_state_rows)
        + direct_path_weight[:, None] * ssm_inputs
    )
    gate_raw = gate_portion.astype(jnp.float32).reshape(sequences, proposals, head_count, head_dim)
    gate_applied_output = (response * jax.nn.silu(gate_raw)).reshape(
        sequences, proposals, group_count, group_inner
    )
    scaled = (
        gate_applied_output
        * rms_scale(gate_applied_output)
        * group_norm_scale.reshape(group_count, group_inner)
    )
    flat_gated = scaled.astype(jnp.bfloat16).reshape(sequences, proposals, head_count * head_dim)
    return (flat_gated, running_state_rows, convolution_span)


def local(
    tokens,
    input_norm_scale,
    head_input_matrix,
    output_gate_matrix,
    group_input_matrix,
    group_readout_matrix,
    step_size_matrix,
    step_size_bias,
    log_decay_rate,
    direct_path_weight,
    convolution_tap_weight,
    convolution_history_rows,
    per_proposal_states,
    accepted,
    proposal_extra_decay,
    group_norm_scale,
    output_projection_matrix,
):
    local_seqs, proposals, width = tokens.shape
    head_local = step_size_bias.shape[0]
    group_local = convolution_tap_weight.shape[1]
    head_dim = per_proposal_states.shape[3]
    state_size = per_proposal_states.shape[4]
    group_inner = head_local // group_local * head_dim
    widened = tokens.astype(jnp.float32)
    normed = (widened * rms_scale(widened) * input_norm_scale).astype(jnp.bfloat16)
    unactivated_step = jnp.einsum(
        "sjd,dh->sjh", normed, step_size_matrix, preferred_element_type=jnp.float32
    )
    pieces = lax.all_to_all(normed, "kv", split_axis=2, concat_axis=0, tiled=True)
    joined = jnp.concatenate(
        [head_input_matrix, group_input_matrix, group_readout_matrix, output_gate_matrix], axis=1
    )
    summed = lax.psum_scatter(
        jnp.einsum("sjd,dc->sjc", pieces, joined, preferred_element_type=jnp.float32),
        "kv",
        scatter_dimension=0,
        tiled=True,
    )
    projected = summed.astype(jnp.bfloat16)
    input_width = head_local * head_dim
    inject_width = group_local * state_size
    part_input = projected[..., :input_width].reshape(
        local_seqs, proposals, group_local, group_inner
    )
    part_inject = projected[..., input_width : input_width + inject_width].reshape(
        local_seqs, proposals, group_local, state_size
    )
    part_readout = projected[
        ..., input_width + inject_width : input_width + 2 * inject_width
    ].reshape(local_seqs, proposals, group_local, state_size)
    gate_portion = projected[..., input_width + 2 * inject_width :]
    incoming_token_rows = jnp.concatenate([part_input, part_inject, part_readout], axis=-1)
    gate_applied_output, running_state_rows, convolution_span = combine_head_outputs(
        incoming_token_rows,
        gate_portion,
        unactivated_step,
        step_size_bias,
        log_decay_rate,
        direct_path_weight,
        convolution_tap_weight,
        convolution_history_rows,
        per_proposal_states,
        accepted,
        proposal_extra_decay,
        group_norm_scale,
    )
    terms = jnp.einsum(
        "sjc,cd->sjd",
        lax.all_gather(gate_applied_output, "kv", axis=0, tiled=True),
        output_projection_matrix,
        preferred_element_type=jnp.float32,
    )
    mixed = lax.psum_scatter(terms.astype(jnp.bfloat16), "tp", scatter_dimension=0, tiled=True)
    return (mixed, running_state_rows, convolution_span)


def solution(mesh):
    return jax.shard_map(
        local,
        mesh=mesh,
        in_specs=(
            P(("grp", "kv"), None, None),
            P(),
            P("kv", "tp"),
            P("kv", "tp"),
            P("kv", "tp"),
            P("kv", "tp"),
            P(None, "tp"),
            P("tp"),
            P("tp"),
            P("tp"),
            P(None, "tp", None),
            P(("grp", "kv"), None, "tp", None),
            P(("grp", "kv"), None, "tp", None, None),
            P(("grp", "kv")),
            P(("grp", "kv"), None, "tp"),
            P("tp"),
            P("tp", "kv"),
        ),
        out_specs=(
            P(("grp", "tp"), None, "kv"),
            P(("grp", "kv"), None, "tp", None, None),
            P(("grp", "kv"), None, "tp", None),
        ),
        check_vma=False,
    )
```

profile of v0, /device:TPU:0, one launch (start us, length us, event | category | flops | bytes accessed | tf_op | source)
XLA Modules:
  0.0 112.8 jit_solution(2285924247131712935)
XLA Ops:
  0.7 0.9 fusion.12
  1.6 0.9 fusion.14
  2.5 2.8 %copy.69 = bf16[1,3,4096]{1,0,2:T(2,128)(2,1)S(1)} copy(bf16[1,3,4096]{2,1,0:T(4,128)(2,1)S(1)} %fusion.14) | data formatting | bytes 49152 | tf_op jit(solution)/shard_map/convert_element_type | solution.py:108
  5.8 22.4 %reduce.15 = bf16[4096,3]{1,0:T(8,128)(2,1)S(1)} reduce(bf16[4096,1,3]{2,1,0:T(2,128)(2,1)S(1)} %bitcast.84, bf16[]{:T(256)} %broadcast.303), dimensions={1}, to_apply=%bitcast.74.reduce_sub_computation | reduce | bytes 49154
  28.3 2.1 %reshape.441 = bf16[4,2,1536]{2,1,0:T(2,128)(2,1)} reshape(bf16[4096,3]{1,0:T(8,128)(2,1)S(1)} %reduce.15) | data formatting | bytes 49152
  30.4 6.3 %all-to-all-start = ((bf16[4,2,1536]{2,1,0:T(2,128)(2,1)}), bf16[4,2,1536]{2,1,0:T(2,128)(2,1)S(1)}, u32[]{:S(2)}, u32[]{:S(2)}) async-start(bf16[4,2,1536]{2,1,0:T(2,128)(2,1)} %reshape.441), calls=%async_computation | async-start | bytes 49152 | tf_op jit(solution)/shard_map/all_to_all | solution.py:112
  39.5 0.8 compare_select_fusion
  40.4 0.7 fusion.23
  41.4 1.3 %fusion.8 = f32[32,64,64]{2,1,0:T(8,128)S(1)} fusion(f32[1,3,32,64,64]{4,3,2,1,0:T(8,128)} %param.29, s32[]{:T(128)} %bitcast.20, pred[]{:T(512)} %bitcast.19), kind=kLoop, calls=%fused_computation.11 | loop fusion | flops 131072 | bytes 1048581 | tf_op jit(solution)/shard_map/jit(take_along_axis)/select_n | solution.py:61
  42.8 1.2 %dynamic-slice.4 = u32[1]{0:T(128)} dynamic-slice(u32[32]{0:T(128)} %constant.86, u32[]{:T(128)S(6)} %add.157), dynamic_slice_sizes={1} | dynamic-slice | bytes 12
  44.0 1.3 %dynamic-slice.6 = u32[1]{0:T(128)} dynamic-slice(u32[32]{0:T(128)} %constant.90, u32[]{:T(128)S(6)} %add.157), dynamic_slice_sizes={1} | dynamic-slice | bytes 12
  45.3 2.1 %reshape.442 = bf16[4096,1,3]{2,1,0:T(2,128)(2,1)S(1)} reshape(bf16[4,2,1536]{2,1,0:T(2,128)(2,1)S(1)} %all-to-all-done) | data formatting | bytes 49152
  47.4 2.0 %copy.70 = bf16[1,3,4096]{2,1,0:T(4,128)(2,1)S(1)} copy(bf16[1,3,4096]{1,0,2:T(2,128)(2,1)S(1)} %bitcast.85) | data formatting | bytes 49152 | tf_op jit(solution)/shard_map/all_to_all | solution.py:112
  49.5 5.0 %fusion = f32[4,3,4352]{2,0,1:T(4,128)S(1)} fusion(bf16[1024,2048]{1,0:T(8,128)(2,1)} %param.20, bf16[1024,128]{1,0:T(8,128)(2,1)} %param.22, bf16[1024,128]{1,0:T(8,128)(2,1)} %param.21, bf16[1024,2048]{1,0:T(8,128)(2,1)} %param.19, bf16[1,3,4,1024]{3,2,1,0:T(4,128)(2,1)S(1)} %all_to_all.14), kind=kOutput, calls=%fused_computation.2 | convolution fusion | flops 142606336 | bytes 9146368 | tf_op jit(solution)/shard_map/sjd,dc->sjc/dot_general | solution.py:117
  54.5 23.6 %all-reduce.3 = bf16[4,3,4352]{2,0,1:T(4,128)(2,1)S(1)} all-reduce(f32[4,3,4352]{2,0,1:T(4,128)S(1)} %fusion), channel_id=2, replica_groups=mesh['grp'=2,'kv'=4,'tp'=4] {'kv'}, use_global_device_ids=true, to_apply=%region_1.0.clone | all-reduce | flops 52224 | bytes 313344
  78.1 0.7 dynamic-slice_convert_fusion
  79.3 0.7 pad_maximum_fusion
  80.4 1.4 %bitcast_add_fusion = f32[1,3,32,64,64]{4,3,1,2,0:T(8,128)S(1)} fusion(bf16[3,32,64,1]{2,0,3,1:T(4,128)(2,1)S(1)} %bitcast.88, f32[32,64,64]{2,1,0:T(8,128)S(1)} %fusion.8, f32[3,32]{0,1:T(8,128)S(1)} %copy.72, f32[3,32,3]{0,2,1:T(4,128)S(1)} %multiply_bitcast_fusion, f32[3,32,64]{2,0,1:T(4,128)S(1)} %copy.73), kind=kOutput, calls=%fused_computation.5 | convolution fusion | flops 3164160 | bytes 2135552 | tf_op jit(solution)/shard_map/sjih,sihp,sihn->sjhpn/dot_general | solution.py:21
  81.8 1.9 %copy.80 = f32[1,3,32,64,64]{4,3,2,1,0:T(8,128)} copy(f32[1,3,32,64,64]{4,3,1,2,0:T(8,128)S(1)} %bitcast_add_fusion) | data formatting | bytes 3145728
  83.7 0.9 fusion.3
  85.2 13.1 %all_gather.3 = bf16[4,3,2048]{2,1,0:T(4,128)(2,1)S(1)} all-gather(bf16[1,3,2048]{2,1,0:T(4,128)(2,1)S(1)} %multiply_convert_fusion), channel_id=1, replica_groups=mesh['grp'=2,'kv'=4,'tp'=4] {'kv'}, dimensions={0}, use_global_device_ids=true | all-gather | bytes 61440 | tf_op jit(solution)/shard_map/all_gather | solution.py:152
  98.4 2.8 %fusion.5 = bf16[4,3,1024]{2,0,1:T(4,128)(2,1)S(1)} fusion(bf16[2048,1024]{1,0:T(8,128)(2,1)} %param.33, bf16[4,3,2048]{2,1,0:T(4,128)(2,1)S(1)} %all_gather.3), kind=kOutput, calls=%fused_computation.8 | convolution fusion | flops 50343936 | bytes 4268032 | tf_op jit(solution)/shard_map/sjc,cd->sjd/dot_general | solution.py:150
  101.2 10.3 %all-reduce.1 = bf16[4,3,1024]{2,1,0:T(4,128)(2,1)S(1)} all-reduce(bf16[4,3,1024]{2,1,0:T(4,128)(2,1)S(1)} %copy.79), channel_id=3, replica_groups=mesh['grp'=2,'kv'=4,'tp'=4] {'tp'}, use_global_device_ids=true, to_apply=%region_5.6.clone | all-reduce | flops 12288 | bytes 49152
  111.5 1.2 %constant_dynamic-slice_fusion = bf16[1,3,1024]{2,1,0:T(4,128)(2,1)} fusion(bf16[4,3,1024]{2,1,0:T(4,128)(2,1)S(1)} %all-reduce.1, u32[]{:T(128)} %bitcast.45), kind=kLoop, calls=%fused_computation.61 | loop fusion | bytes 12292
  (63 shorter events, 4.6 us)
Async XLA Ops:
  0.6 38.8 %copy-start = (bf16[4096,32]{0,1:T(8,128)(2,1)S(1)}, bf16[4096,32]{0,1:T(8,128)(2,1)}, u32[]{:S(2)}) copy-start(bf16[4096,32]{0,1:T(8,128)(2,1)} %param.23) | copy-start | bytes 786436
  0.6 36.8 %copy-start.7 = (bf16[1,6,2,1152]{3,2,1,0:T(2,128)(2,1)S(1)}, bf16[1,6,2,1152]{3,2,1,0:T(2,128)(2,1)}, u32[]{:S(2)}) copy-start(bf16[1,6,2,1152]{3,2,1,0:T(2,128)(2,1)} %param.28) | copy-start | bytes 82948
  0.7 37.5 %copy-start.5 = (bf16[4,2,1152]{2,1,0:T(2,128)(2,1)S(1)}, bf16[4,2,1152]{2,1,0:T(2,128)(2,1)}, u32[]{:S(2)}) copy-start(bf16[4,2,1152]{2,1,0:T(2,128)(2,1)} %param.27) | copy-start | bytes 55300
  30.4 15.0 %all-to-all-start = ((bf16[4,2,1536]{2,1,0:T(2,128)(2,1)}), bf16[4,2,1536]{2,1,0:T(2,128)(2,1)S(1)}, u32[]{:S(2)}, u32[]{:S(2)}) async-start(bf16[4,2,1536]{2,1,0:T(2,128)(2,1)} %reshape.441), calls=%async_computation | async-start | bytes 49152 | tf_op jit(solution)/shard_map/all_to_all | solution.py:112
  49.5 30.5 %copy-start.1 = (f32[2,1152]{1,0:T(2,128)S(1)}, f32[2,1152]{1,0:T(2,128)}, u32[]{:S(2)}) copy-start(f32[2,1152]{1,0:T(2,128)} %get-tuple-element.33) | copy-start | bytes 27652
  49.5 30.5 %copy-start.2 = (f32[2,1152]{1,0:T(2,128)S(1)}, f32[2,1152]{1,0:T(2,128)}, u32[]{:S(2)}) copy-start(f32[2,1152]{1,0:T(2,128)} %get-tuple-element.34) | copy-start | bytes 27652
  49.5 30.5 %copy-start.3 = (f32[2,1152]{1,0:T(2,128)S(1)}, f32[2,1152]{1,0:T(2,128)}, u32[]{:S(2)}) copy-start(f32[2,1152]{1,0:T(2,128)} %get-tuple-element.35) | copy-start | bytes 27652
  49.5 30.5 %copy-start.4 = (f32[2,1152]{1,0:T(2,128)S(1)}, f32[2,1152]{1,0:T(2,128)}, u32[]{:S(2)}) copy-start(f32[2,1152]{1,0:T(2,128)} %get-tuple-element.36) | copy-start | bytes 27652
  81.8 2.8 %copy-start.8 = (f32[32]{0:T(128)S(1)}, f32[32]{0:T(128)}, u32[]{:S(2)}) copy-start(f32[32]{0:T(128)} %param.26) | copy-start | bytes 388
  81.8 3.4 %copy-start.6 = (f32[2048]{0:T(1024)S(1)}, f32[2048]{0:T(1024)}, u32[]{:S(2)}) copy-start(f32[2048]{0:T(1024)} %param.32) | copy-start | bytes 24580
where the time goes:
time: 113 us
  blocking collectives  47 us (42%)
  other arithmetic  28.3 us (25%)
  local copies, waits for them, and re-layouts  18.6 us (16%)
  matrix products  11 us (10%)
  starting transfers between devices  6.35 us (6%)
  between operations  1.59 us (1%)
    unnamed x2, blocking collectives  33.9 us
    unnamed x1, other arithmetic  22.4 us
    all_gather x1, blocking collectives, local(): lax.all_gather(gate_applied_output, 'kv', axis=0, tiled=True)  13.1 us
    unnamed x25, local copies, waits for them, and re-layouts  10.4 us
    all_to_all x1, starting transfers between devices, local(): lax.all_to_all(normed, 'kv', split_axis=2, concat_axis=0, tiled=True)  6.35 us
    dot_general x1, matrix products, local(): jnp.einsum('sjd,dc->sjc', pieces, joined, preferred_element_type=jnp.floa...  4.97 us
    dot_general x1, matrix products, local(): jnp.einsum('sjc,cd->sjd', lax.all_gather(gate_applied_output, 'kv', axis=...  2.85 us
    convert_element_type x1, local copies, waits for them, and re-layouts, local(): (widened * rms_scale(widened) * input_norm_scale).astype(jnp.bfloat16)  2.84 us
  transfers between devices with their start and end apart: 1, of which 0 were waited for; matrix products, arithmetic and copies ran while one was open for 7% of the time, Pallas kernels for 0%

commit v1 on v0

--- a/solution.py
+++ b/solution.py
@@ -109,7 +109,10 @@
     unactivated_step = jnp.einsum(
         "sjd,dh->sjh", normed, step_size_matrix, preferred_element_type=jnp.float32
     )
-    pieces = lax.all_to_all(normed, "kv", split_axis=2, concat_axis=0, tiled=True)
+    pieces = jnp.concatenate(
+        lax.all_to_all(jnp.stack(jnp.split(normed, lax.axis_size("kv"), axis=2)), "kv", 0, 0),
+        axis=0,
+    )
     joined = jnp.concatenate(
         [head_input_matrix, group_input_matrix, group_readout_matrix, output_gate_matrix], axis=1
     )

time: 113 us -> 82.7 us (0.73)
  other arithmetic: 28.3 us -> 6.65 us
  local copies, waits for them, and re-layouts: 18.6 us -> 9.78 us
    unnamed x1 -> x0, other arithmetic: 22.4 us -> none
    unnamed x25 -> x10, local copies, waits for them, and re-layouts: 10.4 us -> 5.76 us
    convert_element_type x1 -> x0, local copies, waits for them, and re-layouts: 2.84 us -> none  [local(): (widened * rms_scale(widened) * input_norm_scale).astype(jnp.bfloat16)]
    all_to_all x2 -> x0, local copies, waits for them, and re-layouts: 2.07 us -> none  [local(): lax.all_to_all(normed, 'kv', split_axis=2, concat_axis=0, tiled=True)]
  transfers between devices with their start and end apart: 1 -> 1, of which waited for: 0 -> 0; matrix products, arithmetic and copies ran while one was open for 7% -> 11% of each run, Pallas kernels for 0% -> 0%
where the time goes in v1:
time: 82.7 us; the launch traced here: 82.1 us
  blocking collectives  46.8 us (57%)
  matrix products  11 us (13%)
  local copies, waits for them, and re-layouts  9.78 us (12%)
  other arithmetic  6.65 us (8%)
  starting transfers between devices  6.35 us (8%)
  between operations  1.51 us (2%)
    unnamed x2, blocking collectives  33.7 us
    all_gather x1, blocking collectives, local(): lax.all_gather(gate_applied_output, 'kv', axis=0, tiled=True)  13.1 us
    all_to_all x1, starting transfers between devices, local(): lax.all_to_all(jnp.stack(jnp.split(normed, lax.axis_size('kv'), axis=2)),...  6.35 us
    unnamed x10, local copies, waits for them, and re-layouts  5.76 us
    dot_general x1, matrix products, local(): jnp.einsum('sjd,dc->sjc', pieces, joined, preferred_element_type=jnp.floa...  4.95 us
    dot_general x1, matrix products, local(): jnp.einsum('sjc,cd->sjd', lax.all_gather(gate_applied_output, 'kv', axis=...  2.85 us
  transfers between devices with their start and end apart: 1, of which 0 were waited for; matrix products, arithmetic and copies ran while one was open for 11% of the time, Pallas kernels for 0%

profile of v1, /device:TPU:0, one launch (start us, length us, event | category | flops | bytes accessed | tf_op | source)
XLA Modules:
  0.0 82.1 jit_solution(12368797726342899108)
XLA Ops:
  0.6 0.9 %fusion.12 = f32[3]{0:T(128)S(1)} fusion(bf16[1,3,4096]{2,1,0:T(4,128)(2,1)} %param.17), kind=kLoop, calls=%fused_computation.17 | loop fusion | flops 36861 | bytes 24588 | tf_op jit(solution)/shard_map/reduce_sum | solution.py:10
  1.6 0.9 %fusion.14 = bf16[1,3,4096]{2,1,0:T(4,128)(2,1)S(1)} fusion(bf16[1,3,4096]{2,1,0:T(4,128)(2,1)} %param.17, f32[4096]{0:T(1024)} %param.18, f32[3]{0:T(128)S(1)} %add_rsqrt_fusion.1), kind=kLoop, calls=%fused_computation.19 | loop fusion | flops 49152 | bytes 65548 | tf_op jit(solution)/shard_map/convert_element_type | solution.py:108
  2.5 0.6 pad_maximum_fusion
  3.1 6.3 %all-to-all-start = ((bf16[4,1,3,1024]{3,2,1,0:T(4,128)(2,1)}), bf16[4,1,3,1024]{3,2,1,0:T(4,128)(2,1)S(1)}, u32[]{:S(2)}, u32[]{:S(2)}) async-start(bf16[4,1,3,1024]{3,2,1,0:T(4,128)(2,1)} %pad_maximum_fusion), calls=%async_computation | async-start | bytes 65536 | tf_op jit(solution)/shard_map/all_to_all | solution.py:113
  10.2 1.3 %gather_fusion = bf16[3,2,1152]{2,1,0:T(2,128)(2,1)S(1)} fusion(bf16[6,2,1152]{2,1,0:T(2,128)(2,1)} %bitcast.91, s32[1024]{0:T(1024)S(1)} %pad_clamp_fusion), kind=kCustom, calls=%fused_computation | custom fusion | bytes 27660 | tf_op jit(solution)/shard_map/jit(take_along_axis)/gather | solution.py:46
  11.7 0.8 bitcast_convert_fusion.3
  12.5 0.7 exp.33
  13.1 0.8 %compare_select_fusion = f32[3,32]{1,0:T(4,128)S(1)} fusion(bf16[4096,32]{0,1:T(8,128)(2,1)S(1)} %copy-done, bf16[1,3,4096]{2,1,0:T(4,128)(2,1)S(1)} %fusion.14, f32[32]{0:T(128)} %param.24), kind=kOutput, calls=%fused_computation.50 | convolution fusion | flops 787104 | bytes 287232 | tf_op jit(solution)/shard_map/sjd,dh->sjh/dot_general | solution.py:109
  14.1 0.7 fusion.24
  15.0 1.3 %fusion.8 = f32[32,64,64]{2,1,0:T(8,128)S(1)} fusion(f32[1,3,32,64,64]{4,3,2,1,0:T(8,128)} %param.29, s32[]{:T(128)} %bitcast.23, pred[]{:T(512)} %bitcast.22), kind=kLoop, calls=%fused_computation.11 | loop fusion | flops 131072 | bytes 1048581 | tf_op jit(solution)/shard_map/jit(take_along_axis)/select_n | solution.py:61
  16.4 1.2 %dynamic-slice.4 = u32[1]{0:T(128)} dynamic-slice(u32[32]{0:T(128)} %constant.86, u32[]{:T(128)S(6)} %add.157), dynamic_slice_sizes={1} | dynamic-slice | bytes 12
  17.7 1.3 %dynamic-slice.6 = u32[1]{0:T(128)} dynamic-slice(u32[32]{0:T(128)} %constant.90, u32[]{:T(128)S(6)} %add.157), dynamic_slice_sizes={1} | dynamic-slice | bytes 12
  19.0 4.9 %fusion = f32[4,3,4352]{2,0,1:T(4,128)S(1)} fusion(bf16[1024,2048]{1,0:T(8,128)(2,1)} %param.20, bf16[1024,128]{1,0:T(8,128)(2,1)} %param.22, bf16[1024,128]{1,0:T(8,128)(2,1)} %param.21, bf16[1024,2048]{1,0:T(8,128)(2,1)} %param.19, bf16[4,1,3,1024]{3,2,1,0:T(4,128)(2,1)S(1)} %all-to-all-done), kind=kOutput, calls=%fused_computation.2 | convolution fusion | flops 142606336 | bytes 9146368 | tf_op jit(solution)/shard_map/sjd,dc->sjc/dot_general | solution.py:120
  23.9 23.4 %all-reduce.3 = bf16[4,3,4352]{2,0,1:T(4,128)(2,1)S(1)} all-reduce(f32[4,3,4352]{2,0,1:T(4,128)S(1)} %fusion), channel_id=2, replica_groups=mesh['grp'=2,'kv'=4,'tp'=4] {'kv'}, use_global_device_ids=true, to_apply=%region_1.0.clone | all-reduce | flops 52224 | bytes 313344
  47.4 0.7 dynamic-slice_convert_fusion
  48.6 0.7 pad_maximum_fusion.1
  49.6 1.4 %bitcast_add_fusion = f32[1,3,32,64,64]{4,3,1,2,0:T(8,128)S(1)} fusion(bf16[3,32,64,1]{2,0,3,1:T(4,128)(2,1)S(1)} %bitcast.90, f32[32,64,64]{2,1,0:T(8,128)S(1)} %fusion.8, f32[3,32]{0,1:T(8,128)S(1)} %copy.94, f32[3,32,3]{0,2,1:T(4,128)S(1)} %multiply_bitcast_fusion, f32[3,32,64]{2,0,1:T(4,128)S(1)} %copy.95), kind=kOutput, calls=%fused_computation.5 | convolution fusion | flops 3164160 | bytes 2135552 | tf_op jit(solution)/shard_map/sjih,sihp,sihn->sjhpn/dot_general | solution.py:21
  51.1 1.9 %copy.102 = f32[1,3,32,64,64]{4,3,2,1,0:T(8,128)} copy(f32[1,3,32,64,64]{4,3,1,2,0:T(8,128)S(1)} %bitcast_add_fusion) | data formatting | bytes 3145728
  53.0 0.9 %fusion.3 = f32[3,32,1,64]{3,2,1,0:T(1,128)S(1)} fusion(f32[3,32,64,1]{2,3,1,0:T(1,128)S(1)} %bitcast.88, f32[1,3,32,64,64]{4,3,1,2,0:T(8,128)S(1)} %bitcast_add_fusion), kind=kOutput, calls=%fused_computation.6 | convolution fusion | flops 786432 | bytes 1622016 | tf_op jit(solution)/shard_map/sjhn,sjhpn->sjhp/dot_general | solution.py:66
  53.9 0.2 multiply_reduce_fusion
  54.5 13.1 %all_gather.3 = bf16[4,3,2048]{2,1,0:T(4,128)(2,1)S(1)} all-gather(bf16[1,3,2048]{2,1,0:T(4,128)(2,1)S(1)} %multiply_convert_fusion), channel_id=1, replica_groups=mesh['grp'=2,'kv'=4,'tp'=4] {'kv'}, dimensions={0}, use_global_device_ids=true | all-gather | bytes 61440 | tf_op jit(solution)/shard_map/all_gather | solution.py:155
  67.6 2.8 %fusion.5 = bf16[4,3,1024]{2,0,1:T(4,128)(2,1)S(1)} fusion(bf16[2048,1024]{1,0:T(8,128)(2,1)} %param.33, bf16[4,3,2048]{2,1,0:T(4,128)(2,1)S(1)} %all_gather.3), kind=kOutput, calls=%fused_computation.8 | convolution fusion | flops 50343936 | bytes 4268032 | tf_op jit(solution)/shard_map/sjc,cd->sjd/dot_general | solution.py:153
  70.5 10.3 %all-reduce.1 = bf16[4,3,1024]{2,1,0:T(4,128)(2,1)S(1)} all-reduce(bf16[4,3,1024]{2,1,0:T(4,128)(2,1)S(1)} %copy.101), channel_id=3, replica_groups=mesh['grp'=2,'kv'=4,'tp'=4] {'tp'}, use_global_device_ids=true, to_apply=%region_5.6.clone | all-reduce | flops 12288 | bytes 49152
  80.8 1.3 %constant_dynamic-slice_fusion = bf16[1,3,1024]{2,1,0:T(4,128)(2,1)} fusion(bf16[4,3,1024]{2,1,0:T(4,128)(2,1)S(1)} %all-reduce.1, u32[]{:T(128)} %bitcast.47), kind=kLoop, calls=%fused_computation.67 | loop fusion | bytes 12292
  (46 shorter events, 2.0 us)
Async XLA Ops:
  0.6 12.5 %copy-start = (bf16[4096,32]{0,1:T(8,128)(2,1)S(1)}, bf16[4096,32]{0,1:T(8,128)(2,1)}, u32[]{:S(2)}) copy-start(bf16[4096,32]{0,1:T(8,128)(2,1)} %param.23) | copy-start | bytes 786436
  3.1 15.9 %all-to-all-start = ((bf16[4,1,3,1024]{3,2,1,0:T(4,128)(2,1)}), bf16[4,1,3,1024]{3,2,1,0:T(4,128)(2,1)S(1)}, u32[]{:S(2)}, u32[]{:S(2)}) async-start(bf16[4,1,3,1024]{3,2,1,0:T(4,128)(2,1)} %pad_maximum_fusion), calls=%async_computation | async-start | bytes 65536 | tf_op jit(solution)/shard_map/all_to_all | solution.py:113
  51.1 2.8 %copy-start.2 = (f32[32]{0:T(128)S(1)}, f32[32]{0:T(128)}, u32[]{:S(2)}) copy-start(f32[32]{0:T(128)} %param.26) | copy-start | bytes 388
  51.1 3.4 %copy-start.1 = (f32[2048]{0:T(1024)S(1)}, f32[2048]{0:T(1024)}, u32[]{:S(2)}) copy-start(f32[2048]{0:T(1024)} %param.32) | copy-start | bytes 24580
